TPU v7x, 32 devices: a whole 2x2x4 slice. The times are simulated.
32 devices in a mesh: sp: 8 (over z, y), tp: 4 (over x, core).
Axes of the slice: x: 2, y: 2, z: 4, core: 2. Of those that a mesh axis runs over, the one named last changes fastest.
Arguments:
- tokens: bfloat16 [6144, 2048], P('sp', 'tp'), may hold values from -18 to 18
- proj_weight: bfloat16 [2048, 1024], P(None, 'tp'), may hold values from -0.125 to 0.125
- gate_weight: bfloat16 [2048, 1024], P(None, 'tp'), may hold values from -0.125 to 0.125
- conv_weight: float32 [4, 1024], replicated, may hold values from -3 to 3
- recur_weight: bfloat16 [16, 64, 64], replicated, may hold values from -0.75 to 0.75
- input_weight: bfloat16 [16, 64, 64], replicated, may hold values from -0.75 to 0.75
- decay_param: float32 [1024], replicated, as said below
- out_grad: bfloat16 [6144, 1024], P('sp', 'tp'), may hold values from -6 to 6
Outputs:
- d_proj: bfloat16 [6144, 1024], P('sp', 'tp')
- d_gate: bfloat16 [6144, 1024], P('sp', 'tp')
- d_weight: float32 [2048, 1024], P('sp', 'tp')
Inputs may be any that keep to these rules, and one draw needn't show every extreme that they name: `decay_param`: every channel's decay parameter is at least 4; there is no fixed upper bound.
All inputs are finite; a program needn't handle non-finite values.
Results may differ from a plain program's by a relative error of at most 0.01.
Values may be sent and summed in bfloat16 or wider, within the bound.
A program may use at most 64 MiB of HBM per device.

v0:
```python
import jax
import jax.numpy as jnp
from jax import lax
from jax.sharding import PartitionSpec as P

BLOCK = 64


rate_scale = 8.0
scale_floor = 0.0001


def from_behind(value, axis, steps):
    count = lax.axis_size(axis)
    first, last = (max(0, -steps), min(count, count - steps))
    return lax.ppermute(value, axis, [(source, source + steps) for source in range(first, last)])


def combine(earlier, later):
    return (earlier[0] * later[0], later[0] * earlier[1] + later[1])


def block_map(values, weights, block_count):
    row_count = values.shape[0]
    shaped = values.reshape(row_count, block_count, BLOCK)
    result = jnp.einsum("tgi,gij->tgj", shaped, weights, preferred_element_type=jnp.float32)
    return result.reshape(row_count, block_count * BLOCK)


def block_back(values, weights, block_count):
    row_count = values.shape[0]
    shaped = values.reshape(row_count, block_count, BLOCK)
    result = jnp.einsum("tgj,gij->tgi", shaped, weights, preferred_element_type=jnp.float32)
    return result.reshape(row_count, block_count * BLOCK)


def per_device(
    tokens, proj_weight, gate_weight, conv_weight, recur_weight, input_weight, decay_param, out_grad
):
    tp_index = lax.axis_index("tp")
    row_count = tokens.shape[0]
    chan_width = proj_weight.shape[1]
    block_count = chan_width // BLOCK
    gathered = lax.all_gather(tokens, "tp", axis=1, tiled=True)
    projected = jnp.dot(gathered, proj_weight, preferred_element_type=jnp.float32).astype(
        jnp.bfloat16
    )
    gate_in = jnp.dot(gathered, gate_weight, preferred_element_type=jnp.float32).astype(
        jnp.bfloat16
    )
    conv_taps = lax.dynamic_slice_in_dim(conv_weight, tp_index * chan_width, chan_width, 1)
    decay_slice = lax.dynamic_slice_in_dim(decay_param, tp_index * chan_width, chan_width, 0)
    w_recur = lax.dynamic_slice_in_dim(recur_weight, tp_index * block_count, block_count, 0)
    w_input = lax.dynamic_slice_in_dim(input_weight, tp_index * block_count, block_count, 0)
    prior_rows = from_behind(projected[row_count - 3 :], "sp", 1)
    padded = jnp.concatenate([prior_rows, projected], axis=0).astype(jnp.float32)
    total = conv_taps[0] * padded[3 : 3 + row_count]
    for offset in range(1, 4):
        total = total + conv_taps[offset] * padded[3 - offset : 3 - offset + row_count]
    conv_out = total.astype(jnp.bfloat16)
    conv_float = conv_out.astype(jnp.float32)
    recur_open = jax.nn.sigmoid(block_map(conv_out, w_recur, block_count))
    input_open = jax.nn.sigmoid(block_map(conv_out, w_input, block_count))
    log_slope = rate_scale * jax.nn.log_sigmoid(decay_slice)
    log_decay = log_slope * recur_open
    decay_rate = jnp.exp(log_decay)
    input_scale = jnp.sqrt(scale_floor - jnp.expm1(2.0 * log_decay))
    gated_input = input_open * conv_float
    drive = input_scale * gated_input
    cum_decay, local_states = lax.associative_scan(combine, (decay_rate, drive), axis=0)
    gelu_gate, gelu_back = jax.vjp(jax.nn.gelu, gate_in.astype(jnp.float32))
    cotangent = out_grad.astype(jnp.float32)
    drive_grad = cotangent * gelu_gate
    shifted = jnp.concatenate([decay_rate[1:], jnp.ones((1, chan_width), jnp.float32)], axis=0)
    cum_after, local_grad = lax.associative_scan(
        combine, (shifted, drive_grad), reverse=True, axis=0
    )
    span_decay = cum_decay[-1]
    span_state = local_states[-1]
    span_grad = decay_rate[0] * local_grad[0]
    all_decay, all_state, all_grad = (
        lax.all_gather(span_decay[None], "sp", axis=0, tiled=True),
        lax.all_gather(span_state[None], "sp", axis=0, tiled=True),
        lax.all_gather(span_grad[None], "sp", axis=0, tiled=True),
    )
    sp_index = lax.axis_index("sp")
    sp_count = lax.axis_size("sp")
    _, fwd_state = lax.associative_scan(combine, (all_decay, all_state), axis=0)
    _, rev_grad = lax.associative_scan(combine, (all_decay, all_grad), reverse=True, axis=0)
    before = lax.dynamic_index_in_dim(fwd_state, jnp.maximum(sp_index - 1, 0), 0, False)
    after = lax.dynamic_index_in_dim(rev_grad, jnp.minimum(sp_index + 1, sp_count - 1), 0, False)
    carry_state = jnp.where(sp_index > 0, before, 0.0)
    carry_grad = jnp.where(sp_index < sp_count - 1, after, 0.0)
    states = local_states + cum_decay * carry_state
    previous = jnp.concatenate([carry_state[None], states[:-1]], axis=0)
    d_gate = gelu_back(cotangent * states)[0].astype(jnp.bfloat16)
    state_grad = local_grad + cum_after * carry_grad
    d_log_decay = state_grad * (
        decay_rate * previous - gated_input * decay_rate * decay_rate / input_scale
    )
    d_recur_pre = (d_log_decay * log_slope * recur_open * (1.0 - recur_open)).astype(jnp.bfloat16)
    d_input_pre = (state_grad * input_scale * conv_float * input_open * (1.0 - input_open)).astype(
        jnp.bfloat16
    )
    d_conv = state_grad * input_scale * input_open
    d_conv = d_conv + block_back(d_recur_pre, w_recur, block_count)
    d_conv = d_conv + block_back(d_input_pre, w_input, block_count)
    next_rows = from_behind(d_conv[:3], "sp", -1)
    extended = jnp.concatenate([d_conv, next_rows], axis=0)
    grad_sum = conv_taps[0] * extended[0:row_count]
    for offset in range(1, 4):
        grad_sum = grad_sum + conv_taps[offset] * extended[offset : offset + row_count]
    d_proj = grad_sum.astype(jnp.bfloat16)
    d_weight = lax.psum_scatter(
        lax.dot_general(
            gathered, d_proj, (((0,), (0,)), ((), ())), preferred_element_type=jnp.float32
        ),
        "sp",
        scatter_dimension=0,
        tiled=True,
    )
    return (d_proj, d_gate, d_weight)


def solution(mesh):
    in_specs = (P("sp", "tp"), P(None, "tp"), P(None, "tp"), P(), P(), P(), P(), P("sp", "tp"))
    out_specs = (P("sp", "tp"), P("sp", "tp"), P("sp", "tp"))
    return jax.shard_map(
        per_device, mesh=mesh, in_specs=in_specs, out_specs=out_specs, check_vma=False
    )
```

profile of v0, /device:TPU:0, one launch (start us, length us, event | category | flops | bytes accessed | tf_op | source)
XLA Modules:
  0.0 441.6 jit_solution(7558327511127030171)
XLA Ops:
  8.9 31.9 %all-gather.5.cloned.1.call-done = bf16[768,2048]{1,0:T(8,128)(2,1)} async-done(((bf16[768,512]{1,0:T(8,128)(2,1)}), bf16[768,2048]{1,0:T(8,128)(2,1)}) %all-gather.5.cloned.1.call-update) | async-done | bytes 3145744 | tf_op jit(solution)/shard_map/all_gather | solution.py:44
  40.8 3.1 convolution_convert_fusion
  44.0 3.4 collective-permute-start
  53.6 2.0 fusion.38
  57.1 3.2 slice.964
  60.3 3.2 slice.924
  63.5 3.2 slice.923
  71.6 2.2 multiply_add_fusion.2
  75.1 1.7 slice.962
  81.4 1.7 slice.894
  86.4 1.9 multiply_add_fusion.4
  124.2 2.0 pad.329
  126.2 2.0 pad.305
  136.1 2.1 pad.330
  138.2 2.1 pad.331
  140.3 2.1 pad.307
  145.5 1.8 fusion.44
  151.0 2.3 pad.333
  153.2 2.3 pad.309
  155.5 1.7 add.563
  157.3 1.7 add.601
  159.0 2.1 fusion.42
  161.8 2.5 pad.310
  165.9 2.5 pad.334
  168.3 2.5 pad.335
  170.8 2.5 pad.311
  173.3 2.0 add.564
  175.3 1.9 add.603
  177.2 2.5 fusion.40
  180.5 2.9 pad.336
  183.4 3.0 pad.337
  187.1 21.3 %all-gather.2 = f32[8,1,256]{2,1,0:T(1,128)S(1)} all-gather(f32[1,1,256]{2,1,0:T(1,128)S(1)} %add_bitcast_fusion), channel_id=1, replica_groups=mesh['sp'=8,'tp'=4] {'sp'}, dimensions={0}, use_global_device_ids=true | all-gather | bytes 9216 | tf_op jit(solution)/shard_map/all_gather | solution.py:83
  208.4 1.8 pad_maximum_fusion.2
  210.2 2.9 pad.312
  213.2 2.9 pad.313
  216.7 16.5 %all-gather.1 = f32[8,1,256]{2,1,0:T(1,128)S(1)} all-gather(f32[1,1,256]{2,1,0:T(1,128)S(1)} %add_bitcast_fusion.1), channel_id=1, replica_groups=mesh['sp'=8,'tp'=4] {'sp'}, dimensions={0}, use_global_device_ids=true | all-gather | bytes 9216 | tf_op jit(solution)/shard_map/all_gather | solution.py:82
  233.7 5.5 %fusion.12 = (bf16[768,256]{1,0:T(8,128)(2,1)}, f32[768,256]{1,0:T(8,128)}, f32[768,256]{1,0:T(8,128)S(1)}) fusion(bf16[768,256]{1,0:T(8,128)(2,1)} %param.15, f32[256]{0:T(256)S(1)} %bitcast.89, f32[768,256]{1,0:T(8,128)} %pad.312, f32[768,256]{1,0:T(8,128)} %pad.313, f32[768,256]{1,0:T(8,128)} %pad.336, f32[768,256]{1,0:T(8,128)} %pad.337, ...), kind=kOutput, calls=%fused_computation.29 | convolution fusion | flops 811204608 | bytes 9700352 | tf_op jit(solution)/shard_map/dot_general | solution.py:48
  240.1 3.2 slice.834
  243.3 3.1 slice.768
  246.4 3.1 slice.766
  254.1 3.9 slice.767
  258.0 3.8 slice.769
  261.8 3.8 slice.772
  265.6 3.8 slice.765
  278.7 2.1 slice.835
  280.8 4.0 slice.763
  292.5 2.5 pad.293
  294.9 2.5 pad.275
  297.4 1.8 add.545
  299.2 1.8 add.555
  301.0 2.3 add_multiply_fusion.2
  305.2 3.0 pad.277
  310.1 18.3 %all-gather = f32[8,1,256]{2,1,0:T(1,128)S(1)} all-gather(f32[1,1,256]{2,1,0:T(1,128)S(1)} %fusion.85), channel_id=1, replica_groups=mesh['sp'=8,'tp'=4] {'sp'}, dimensions={0}, use_global_device_ids=true | all-gather | bytes 9216 | tf_op jit(solution)/shard_map/all_gather | solution.py:84
  328.9 1.8 concatenate.151
  331.4 2.9 pad.294
  334.3 3.0 pad.295
  337.2 2.4 add.556
  339.6 6.8 %rev.14 = f32[768,256]{1,0:T(8,128)} reverse(f32[768,256]{1,0:T(8,128)} %add.556), dimensions={0} | reverse | bytes 1572864 | tf_op jit(solution)/shard_map/rev | solution.py:75
  346.5 3.7 fusion.9
  352.8 1.9 copy.49
  360.0 4.2 collective-permute-done.1
  364.6 2.3 convolution_bitcast_fusion
  366.9 66.0 %reduce-scatter.2.cloned.1.call-done = f32[256,256]{0,1:T(8,128)} async-done(((f32[2048,256]{0,1:T(8,128)}), f32[256,256]{0,1:T(8,128)}) %reduce-scatter.2.cloned.1.call-update) | async-done | bytes 262160 | tf_op jit(solution)/shard_map/reduce_scatter | solution.py:114
  432.9 1.8 copy.57
  (407 shorter events, 113.8 us)
Async XLA Ops:
  7.2 226.6 %copy-start = (bf16[2048,256]{1,0:T(8,128)(2,1)S(1)}, bf16[2048,256]{1,0:T(8,128)(2,1)}, u32[]{:S(2)}) copy-start(bf16[2048,256]{1,0:T(8,128)(2,1)} %param.10) | copy-start | bytes 3145732
  7.2 33.6 %all-gather.5.cloned.1.call-start = ((), (), s32[]{:S(2)}) async-start(), calls=%async_computation.1 | async-start | bytes 3932160 | tf_op jit(solution)/shard_map/all_gather | solution.py:44
  7.9 425.0 %reduce-scatter.2.cloned.1.call-start = ((), (), s32[]{:S(2)}) async-start(), calls=%async_computation.2 | async-start | bytes 2359296 | tf_op jit(solution)/shard_map/reduce_scatter | solution.py:114
  8.9 44.7 %copy-start.14 = (f32[1,256]{1,0:T(1,128)}, f32[1,256]{1,0:T(1,128)S(1)}, u32[]{:S(2)}) copy-start(f32[1,256]{1,0:T(1,128)S(1)} %get-tuple-element.76) | copy-start | bytes 3076
  8.9 44.7 %copy-start.16 = (f32[1,256]{1,0:T(1,128)}, f32[1,256]{1,0:T(1,128)S(1)}, u32[]{:S(2)}) copy-start(f32[1,256]{1,0:T(1,128)S(1)} %get-tuple-element.77) | copy-start | bytes 3076
  8.9 44.7 %copy-start.18 = (f32[1,256]{1,0:T(1,128)}, f32[1,256]{1,0:T(1,128)S(1)}, u32[]{:S(2)}) copy-start(f32[1,256]{1,0:T(1,128)S(1)} %get-tuple-element.78) | copy-start | bytes 3076
  8.9 44.6 %copy-start.20 = (f32[1,256]{1,0:T(1,128)}, f32[1,256]{1,0:T(1,128)S(1)}, u32[]{:S(2)}) copy-start(f32[1,256]{1,0:T(1,128)S(1)} %get-tuple-element.79) | copy-start | bytes 3076
  44.0 4.7 %collective-permute-start = (bf16[3,256]{1,0:T(4,128)(2,1)S(1)}, bf16[3,256]{1,0:T(4,128)(2,1)S(1)}, u32[]{:S(2)}, u32[]{:S(2)}) collective-permute-start(bf16[3,256]{1,0:T(4,128)(2,1)S(1)} %slice.991), channel_id=1, source_target_pairs={{0,4},{4,8},{8,12},{12,16},{16,20},{20,24},{24,28},{1,5},{5,9},{9,... | collective-permute-start | bytes 4616 | tf_op jit(solution)/shard_map/ppermute | solution.py:16
  48.1 5.4 %copy-start.22 = (f32[256]{0:T(256)}, f32[256]{0:T(256)S(1)}, u32[]{:S(2)}) copy-start(f32[256]{0:T(256)S(1)} %fusion.82) | copy-start | bytes 3076
  49.3 1.4 copy-start.13
  55.6 0.9 copy-start.3
  73.8 0.7 copy-start.6
  88.4 0.7 copy-start.10
  101.4 0.6 copy-start.12
  120.2 27.1 %copy-start.29 = (f32[1,256]{1,0:T(1,128)S(1)}, f32[1,256]{1,0:T(1,128)}, u32[]{:S(2)}) copy-start(f32[1,256]{1,0:T(1,128)} %slice.1054) | copy-start | bytes 3076
  120.2 28.5 %copy-start.28 = (f32[1,256]{1,0:T(1,128)S(1)}, f32[1,256]{1,0:T(1,128)}, u32[]{:S(2)}) copy-start(f32[1,256]{1,0:T(1,128)} %slice.1094) | copy-start | bytes 3076
  134.7 26.4 %copy-start.27 = (f32[1,256]{1,0:T(1,128)S(1)}, f32[1,256]{1,0:T(1,128)}, u32[]{:S(2)}) copy-start(f32[1,256]{1,0:T(1,128)} %slice.1053) | copy-start | bytes 3076
  143.9 20.3 %copy-start.26 = (f32[1,256]{1,0:T(1,128)S(1)}, f32[1,256]{1,0:T(1,128)}, u32[]{:S(2)}) copy-start(f32[1,256]{1,0:T(1,128)} %slice.1093) | copy-start | bytes 3076
  170.8 8.8 %copy-start.25 = (f32[1,256]{1,0:T(1,128)S(1)}, f32[1,256]{1,0:T(1,128)}, u32[]{:S(2)}) copy-start(f32[1,256]{1,0:T(1,128)} %slice.1092) | copy-start | bytes 3076
  177.2 31.2 %copy-start.24 = (f32[1,256]{1,0:T(1,128)S(1)}, f32[1,256]{1,0:T(1,128)}, u32[]{:S(2)}) copy-start(f32[1,256]{1,0:T(1,128)} %slice.1049) | copy-start | bytes 3076
  233.7 5.5 %copy-start.30 = (f32[1,256]{1,0:T(1,128)}, f32[1,256]{1,0:T(1,128)S(1)}, u32[]{:S(2)}) copy-start(f32[1,256]{1,0:T(1,128)S(1)} %broadcast_select_fusion) | copy-start | bytes 3076
  239.2 0.9 copy-start.7
  273.3 5.4 %copy-start.8 = (f32[383,256]{1,0:T(8,128)S(1)}, f32[383,256]{1,0:T(8,128)}, u32[]{:S(2)}) copy-start(f32[383,256]{1,0:T(8,128)} %slice.834) | copy-start | bytes 1176580
  285.2 4.5 %copy-start.11 = (f32[191,256]{1,0:T(8,128)S(1)}, f32[191,256]{1,0:T(8,128)}, u32[]{:S(2)}) copy-start(f32[191,256]{1,0:T(8,128)} %slice.773) | copy-start | bytes 586756
  331.3 15.1 %copy-start.2 = (f32[768,256]{1,0:T(8,128)S(1)}, f32[768,256]{1,0:T(8,128)}, u32[]{:S(2)}) copy-start(f32[768,256]{1,0:T(8,128)} %copy.43) | copy-start | bytes 2359300
  331.3 15.1 %copy-start.15 = (f32[1,256]{1,0:T(1,128)S(1)}, f32[1,256]{1,0:T(1,128)}, u32[]{:S(2)}) copy-start(f32[1,256]{1,0:T(1,128)} %copy-done.14) | copy-start | bytes 3076
  331.3 15.1 %copy-start.17 = (f32[1,256]{1,0:T(1,128)S(1)}, f32[1,256]{1,0:T(1,128)}, u32[]{:S(2)}) copy-start(f32[1,256]{1,0:T(1,128)} %copy-done.16) | copy-start | bytes 3076
  331.3 15.1 %copy-start.19 = (f32[1,256]{1,0:T(1,128)S(1)}, f32[1,256]{1,0:T(1,128)}, u32[]{:S(2)}) copy-start(f32[1,256]{1,0:T(1,128)} %copy-done.18) | copy-start | bytes 3076
  331.3 15.1 %copy-start.21 = (f32[1,256]{1,0:T(1,128)S(1)}, f32[1,256]{1,0:T(1,128)}, u32[]{:S(2)}) copy-start(f32[1,256]{1,0:T(1,128)} %copy-done.20) | copy-start | bytes 3076
  331.3 15.1 %copy-start.23 = (f32[256]{0:T(256)S(1)}, f32[256]{0:T(256)}, u32[]{:S(2)}) copy-start(f32[256]{0:T(256)} %copy-done.22) | copy-start | bytes 3076
  331.4 15.1 %copy-start.31 = (f32[1,256]{1,0:T(1,128)S(1)}, f32[1,256]{1,0:T(1,128)}, u32[]{:S(2)}) copy-start(f32[1,256]{1,0:T(1,128)} %copy-done.30) | copy-start | bytes 3076
  351.3 5.8 %copy-start.5 = (f32[768,256]{1,0:T(8,128)S(1)}, f32[768,256]{1,0:T(8,128)}, u32[]{:S(2)}) copy-start(f32[768,256]{1,0:T(8,128)} %get-tuple-element.17) | copy-start | bytes 2359300
  357.1 7.4 %copy-start.4 = (bf16[768,2048]{1,0:T(8,128)(2,1)S(1)}, bf16[768,2048]{1,0:T(8,128)(2,1)}, u32[]{:S(2)}) copy-start(bf16[768,2048]{1,0:T(8,128)(2,1)} %all-gather.5.cloned.1.call-done) | copy-start | bytes 9437188
  358.7 5.5 %collective-permute-start.1 = (f32[3,256]{1,0:T(4,128)S(1)}, f32[3,256]{1,0:T(4,128)S(1)}, u32[]{:S(2)}, u32[]{:S(2)}) collective-permute-start(f32[3,256]{1,0:T(4,128)S(1)} %slice.1134), channel_id=1, source_target_pairs={{4,0},{8,4},{12,8},{16,12},{20,16},{24,20},{28,24},{5,1},{9,5},{13... | collective-permute-start | bytes 9224 | tf_op jit(solution)/shard_map/ppermute | solution.py:16
  364.2 70.5 %copy-start.1 = (bf16[2048,256]{1,0:T(8,128)(2,1)S(1)}, bf16[2048,256]{1,0:T(8,128)(2,1)}, u32[]{:S(2)}) copy-start(bf16[2048,256]{1,0:T(8,128)(2,1)} %param.10) | copy-start | bytes 3145732
  364.6 2.3 copy-start.9
Sparse Core Ops, SparseCore 0:
  9.6 31.2 all-gather.4
  367.0 65.8 reduce-scatter.1
where the time goes:
time: 447 us; the launch traced here: 442 us
  local copies, waits for them, and re-layouts  172 us (38%)
  waiting for transfers between devices  103 us (23%)
  other arithmetic  73.5 us (16%)
  blocking collectives  56.1 us (13%)
  matrix products  16.1 us (4%)
  between operations  15.5 us (3%)
  starting transfers between devices  4.75 us (1%)
    reduce_scatter x1, waiting for transfers between devices, per_device(): lax.psum_scatter(lax.dot_general(gathered, d_proj, (((0,), (0,)), ((), ()...  66 us
    slice x63, local copies, waits for them, and re-layouts, per_device(): lax.associative_scan(combine, (decay_rate, drive), axis=0)  51 us
    slice x69, local copies, waits for them, and re-layouts, per_device(): lax.associative_scan(combine, (shifted, drive_grad), reverse=True, axis=0)  41.5 us
    pad x34, local copies, waits for them, and re-layouts, per_device(): lax.associative_scan(combine, (decay_rate, drive), axis=0)  40.1 us
    all_gather x1, waiting for transfers between devices, per_device(): gathered = lax.all_gather(tokens, 'tp', axis=1, tiled=True)  31.9 us
    all_gather x1, blocking collectives, per_device(): lax.all_gather(span_state[None], 'sp', axis=0, tiled=True)  21.3 us
    all_gather x1, blocking collectives, per_device(): lax.all_gather(span_grad[None], 'sp', axis=0, tiled=True)  18.3 us
    add x22, other arithmetic, combine(): return (earlier[0] * later[0], later[0] * earlier[1] + later[1])  17.5 us
  transfers between devices with their start and end apart: 4, of which 4 were waited for; matrix products, arithmetic and copies ran while one was open for 0% of the time, Pallas kernels for 0%

commit v1 on v0

v1 whole, which is shorter than its diff:
```python
import functools

import jax
import jax.numpy as jnp
from jax import lax
from jax.experimental import pallas as pl
from jax.experimental.pallas import tpu as pltpu
from jax.sharding import PartitionSpec as P

BLOCK = 64
rate_scale = 8.0
scale_floor = 0.0001

SUBS = 8
STEP = 16
LANES = 128
PAD = 8
MESH = pl.DeviceIdType.MESH
F32 = jnp.float32
BF16 = jnp.bfloat16


def mm(a, b, dims=(((1,), (0,)), ((), ()))):
    return lax.dot_general(a, b, dims, preferred_element_type=F32)


def kernel(
    tok_hbm, wp_hbm, wg_hbm, cw_ref, wr_ref, wi_ref, dp_ref, og_hbm,
    dproj_ref, dgate_ref, dw_ref,
    gath, wp, wg, og, wblk, proj, gin, pre,
    dec, drv, dgr, qg, ro_s, io_s, cv_s, sc_s, rs_s, xp, cp, gs, as_,
    ends, carry_k, carry_l, slope_s, taps_s,
    halo_out, halo_in, car_out, car_in, dri, dc, dc_in, dpt, sbuf, rbuf, own,
    loc_sem, ag_send, ag_recv, halo_send, halo_recv, car_send, car_recv,
    dc_send, dc_recv, rs_send, rs_recv,
    *, sp_n, tp_n,
):
    sp = lax.axis_index("sp")
    tp = lax.axis_index("tp")
    core = lax.rem(tp, 2)
    chip = lax.div(tp, 2)
    chips = tp_n // 2
    partner = tp + 1 - 2 * core
    sub_rows = gath.shape[2]
    feat = gath.shape[3]
    chan = wp.shape[1]
    halves = chan // LANES
    pitch = sub_rows + PAD
    chunks = sub_rows // STEP
    rows = SUBS * sub_rows
    groups = chan // BLOCK

    loc = [
        pltpu.make_async_copy(tok_hbm, gath.at[0], loc_sem.at[0]),
        pltpu.make_async_copy(wp_hbm, wp, loc_sem.at[1]),
        pltpu.make_async_copy(wg_hbm, wg, loc_sem.at[2]),
        pltpu.make_async_copy(og_hbm, og, loc_sem.at[3]),
    ]
    for item in loc:
        item.start()

    def sp_at(j):
        return lax.rem(sp + j, sp_n)

    def chip_at(j):
        return lax.rem(chip + j, chips)

    barrier = pltpu.get_barrier_semaphore()
    pl.semaphore_signal(barrier, inc=1, device_id=(sp, partner), device_id_type=MESH)
    for j in range(1, chips):
        pl.semaphore_signal(
            barrier, inc=1, device_id=(sp, chip_at(j) * 2 + core), device_id_type=MESH
        )

    def greet(j, _):
        pl.semaphore_signal(barrier, inc=1, device_id=(sp_at(j), tp), device_id_type=MESH)
        return 0

    lax.fori_loop(1, sp_n, greet, 0)

    cols = pl.ds(pl.multiple_of(tp * chan, chan), chan)
    z = jnp.exp(-dp_ref[:, cols])
    log1p = z * (1.0 - z * (1.0 / 2 - z * (1.0 / 3 - z * (1.0 / 4 - z * (1.0 / 5)))))
    slope_s[...] = -rate_scale * log1p
    taps_s[...] = cw_ref[:, cols]
    wblk[...] = jnp.zeros_like(wblk)
    for g in range(groups):
        at = slice(g * BLOCK, (g + 1) * BLOCK)
        wblk[at, at] = wr_ref[tp * groups + g]
        wblk[at, chan + g * BLOCK : chan + (g + 1) * BLOCK] = wi_ref[tp * groups + g]

    pl.semaphore_wait(barrier, chips + sp_n - 1)
    loc[0].wait()

    def part(c):
        return pl.ds(pl.multiple_of(c * STEP, STEP), STEP)

    def ag_copy(slot, source, c, target):
        return pltpu.make_async_remote_copy(
            src_ref=gath.at[source, :, part(c), :],
            dst_ref=gath.at[slot, :, part(c), :],
            send_sem=ag_send.at[slot, c],
            recv_sem=ag_recv.at[slot, c],
            device_id=(sp, target),
            device_id_type=MESH,
        )

    def cross(j, c):
        return ag_copy(2 * j, 0, c, chip_at(j) * 2 + core)

    def inside(j, c):
        return ag_copy(2 * j + 1, 2 * j, c, partner)

    def send_own(k, _):
        c = lax.rem(k + chunks - 1, chunks)
        for j in range(1, chips):
            cross(j, c).start()
        inside(0, c).start()
        return 0

    lax.fori_loop(0, chunks, send_own, 0)
    for item in loc[1:]:
        item.wait()

    def relay(c):
        for j in range(1, chips):
            cross(j, c).wait_recv()
            inside(j, c).start()

    def project(c):
        acc_p = acc_g = None
        for j in range(chips):
            for other in range(2):
                rel = 2 * j + other
                if other:
                    inside(j, c).wait_recv()
                shard = lax.rem(chip + chips - j, chips) * 2 + (1 - core if other else core)
                x = gath[rel, :, part(c), :].reshape(SUBS * STEP, feat)
                wrows = pl.ds(pl.multiple_of(shard * feat, feat), feat)
                a = mm(x, wp[wrows, :])
                b = mm(x, wg[wrows, :])
                acc_p = a if acc_p is None else acc_p + a
                acc_g = b if acc_g is None else acc_g + b
        shape = (SUBS, STEP, chan)
        proj[:, pl.ds(pl.multiple_of(c * STEP + PAD, PAD), STEP), :] = (
            acc_p.astype(BF16).astype(F32).reshape(shape)
        )
        gin[:, part(c), :] = acc_g.astype(BF16).astype(F32).reshape(shape)

    def gates(c):
        def conv(s, _):
            x = proj[s, pl.ds(pl.multiple_of(c * STEP, PAD), STEP + PAD), :]
            total = taps_s[0:1, :] * x[PAD:]
            for k in range(1, 4):
                total = total + taps_s[k : k + 1, :] * pltpu.roll(x, k, 0)[PAD:]
            dri[pl.ds(pl.multiple_of(s * STEP, STEP), STEP), 0:chan] = total.astype(BF16)
            return 0

        lax.fori_loop(0, SUBS, conv, 0, unroll=4)
        pre[...] = mm(dri[0 : SUBS * STEP, 0:chan], wblk[...])

        def element(s, _):
            at = pl.ds(pl.multiple_of(s * STEP, STEP), STEP)
            to = pl.ds(pl.multiple_of(s * pitch + c * STEP, PAD), STEP)
            src = pl.ds(pl.multiple_of(s * sub_rows + c * STEP, STEP), STEP)
            for h in range(halves):
                lane = slice(h * LANES, (h + 1) * LANES)
                slope = slope_s[:, lane]
                cv = dri[at, lane].astype(F32)
                ro = 0.5 * jnp.tanh(0.5 * pre[at, lane]) + 0.5
                io = 0.5 * jnp.tanh(0.5 * pre[at, chan + h * LANES : chan + (h + 1) * LANES]) + 0.5
                ld = slope * ro
                d = jnp.exp(ld)
                y = 2.0 * ld
                poly = 1.0 + y * (1.0 / 8)
                for m in range(7, 1, -1):
                    poly = 1.0 + (y * (1.0 / m)) * poly
                u = scale_floor - y * poly
                rs = lax.rsqrt(u)
                sc = u * rs
                x = gin[s, part(c), lane]
                cot = og[src, lane].astype(F32)
                x2 = x * x
                th = jnp.tanh(0.7978845608028654 * (x + 0.044715 * (x2 * x)))
                half_up = 0.5 * (1.0 + th)
                slope_g = half_up + 0.5 * x * (1.0 - th * th) * (
                    0.7978845608028654 * (1.0 + 0.134145 * x2)
                )
                dec[h, to, :] = d
                drv[h, to, :] = sc * (io * cv)
                dgr[h, to, :] = cot * (x * half_up)
                qg[h, to, :] = cot * slope_g
                ro_s[h, to, :] = ro
                io_s[h, to, :] = io
                cv_s[h, to, :] = cv
                sc_s[h, to, :] = sc
                rs_s[h, to, :] = rs
            return 0

        lax.fori_loop(0, SUBS, element, 0, unroll=4)

    halo = pltpu.make_async_remote_copy(
        src_ref=halo_out, dst_ref=halo_in, send_sem=halo_send, recv_sem=halo_recv,
        device_id=(sp_at(1), tp), device_id_type=MESH,
    )
    relay(chunks - 1)
    project(chunks - 1)
    halo_out[...] = proj[SUBS - 1, sub_rows:pitch, :]
    halo.start()
    for s in range(1, SUBS):
        proj[s, 0:PAD, :] = proj[s - 1, sub_rows:pitch, :]
    relay(0)
    project(0)
    halo.wait()
    proj[0, 0:PAD, :] = jnp.where(sp > 0, halo_in[...], 0.0)

    def stream(c, _):
        relay(c)
        gates(c - 1)
        project(c)
        return 0

    lax.fori_loop(1, chunks - 1, stream, 0)

    def rest(c, _):
        gates(c)
        return 0

    lax.fori_loop(chunks - 2, chunks, rest, 0)

    one = jnp.ones((SUBS, LANES), F32)
    zero = jnp.zeros((SUBS, LANES), F32)

    def scan(i, state):
        out = []
        fwd = pl.ds(i, SUBS, stride=pitch)
        rev = pl.ds(sub_rows - 1 - i, SUBS, stride=pitch)
        for h in range(halves):
            x, c, g, a = state[4 * h : 4 * h + 4]
            d = dec.at[h][fwd, :]
            xp.at[h][fwd, :] = x
            cp.at[h][fwd, :] = c
            x = d * x + drv.at[h][fwd, :]
            c = c * d
            e = dec.at[h][rev, :]
            g = g + dgr.at[h][rev, :]
            gs.at[h][rev, :] = g
            as_.at[h][rev, :] = a
            g = e * g
            a = a * e
            out += [x, c, g, a]
        return tuple(out)

    final = lax.fori_loop(0, sub_rows, scan, (zero, one, zero, one) * halves, unroll=4)
    for h in range(halves):
        lane = slice(h * LANES, (h + 1) * LANES)
        ends[0, :, lane] = final[4 * h + 1]
        ends[1, :, lane] = final[4 * h]
        ends[2, :, lane] = final[4 * h + 2]
    p_list, q_list, b_list, e_list = [], [], [None] * SUBS, [None] * SUBS
    p = jnp.zeros((1, chan), F32)
    q = jnp.ones((1, chan), F32)
    for s in range(SUBS):
        p_list.append(p)
        q_list.append(q)
        p = ends[0, s : s + 1, :] * p + ends[1, s : s + 1, :]
        q = ends[0, s : s + 1, :] * q
    b = jnp.zeros((1, chan), F32)
    e = jnp.ones((1, chan), F32)
    for s in range(SUBS - 1, -1, -1):
        b_list[s] = b
        e_list[s] = e
        b = ends[0, s : s + 1, :] * b + ends[2, s : s + 1, :]
        e = ends[0, s : s + 1, :] * e
    car_out[0:1, :] = q
    car_out[1:2, :] = p
    car_out[2:3, :] = b
    car_out[3:8, :] = jnp.zeros((5, chan), F32)

    def car_copy(j):
        return pltpu.make_async_remote_copy(
            src_ref=car_out, dst_ref=car_in.at[j], send_sem=car_send.at[j],
            recv_sem=car_recv.at[j], device_id=(sp_at(j), tp), device_id_type=MESH,
        )

    def car_start(j, _):
        car_copy(j).start()
        return 0

    def car_wait(j, _):
        car_copy(j).wait()
        return 0

    lax.fori_loop(1, sp_n, car_start, 0)
    lax.fori_loop(1, sp_n, car_wait, 0)

    def join(m, state):
        cs, cg = state
        j = sp_n - m
        cs = jnp.where(j <= sp, car_in[j, 0:1, :] * cs + car_in[j, 1:2, :], cs)
        cg = jnp.where(sp + j < sp_n, car_in[m, 0:1, :] * cg + car_in[m, 2:3, :], cg)
        return cs, cg

    nothing = jnp.zeros((1, chan), F32)
    cs, cg = lax.fori_loop(1, sp_n, join, (nothing, nothing))
    for s in range(SUBS):
        carry_k[s] = p_list[s] + q_list[s] * cs
        carry_l[s] = b_list[s] + e_list[s] * cg

    def back(s):
        base = pl.multiple_of(s * pitch, PAD)
        outb = pl.multiple_of(s * sub_rows, STEP)
        for r in range(0, sub_rows, STEP):
            at = pl.ds(base + r, STEP)
            to = pl.ds(outb + r, STEP)
            for h in range(halves):
                lane = slice(h * LANES, (h + 1) * LANES)
                kk = carry_k[s, :, lane]
                ll = carry_l[s, :, lane]
                d = dec[h, at, :]
                prev = xp[h, at, :] + cp[h, at, :] * kk
                dp = d * prev
                dgate_ref[to, lane] = (qg[h, at, :] * (dp + drv[h, at, :])).astype(BF16)
                sg = gs[h, at, :] + as_[h, at, :] * ll
                ro, io, cv, sc = ro_s[h, at, :], io_s[h, at, :], cv_s[h, at, :], sc_s[h, at, :]
                dld = sg * (dp - io * cv * d * d * rs_s[h, at, :])
                dr = dld * slope_s[:, lane] * ro * (1.0 - ro)
                sgi = sg * sc * io
                di = sgi * cv * (1.0 - io)
                dri[r : r + STEP, lane] = dr.astype(BF16)
                dri[r : r + STEP, chan + h * LANES : chan + (h + 1) * LANES] = di.astype(BF16)
                dc[to, lane] = sgi
        whole = pl.ds(outb, sub_rows)
        dc[whole, :] += mm(dri[0:sub_rows, :], wblk[...], (((1,), (1,)), ((), ())))

    back(0)
    halo_out[...] = dc[0:PAD, :]
    dc_copy = pltpu.make_async_remote_copy(
        src_ref=halo_out, dst_ref=dc_in, send_sem=dc_send, recv_sem=dc_recv,
        device_id=(sp_at(sp_n - 1), tp), device_id_type=MESH,
    )
    dc_copy.start()

    def back_step(s, _):
        back(s)
        return 0

    lax.fori_loop(1, SUBS, back_step, 0)
    dc_copy.wait()
    dc[rows : rows + PAD, :] = jnp.where(sp < sp_n - 1, dc_in[...], 0.0)

    def unconv(i, _):
        r = pl.multiple_of(i * STEP, STEP)
        x = dc[pl.ds(r, STEP + PAD), :]
        total = taps_s[0:1, :] * x[:STEP]
        for k in range(1, 4):
            total = total + taps_s[k : k + 1, :] * pltpu.roll(x, STEP + PAD - k, 0)[:STEP]
        dproj_ref[pl.ds(r, STEP), :] = total.astype(BF16)
        return 0

    lax.fori_loop(0, rows // STEP, unconv, 0, unroll=4)

    piece = feat * tp_n // sp_n
    flip = piece % LANES == 0

    def rs_copy(j):
        return pltpu.make_async_remote_copy(
            src_ref=sbuf.at[j if flip else sp_at(j)], dst_ref=rbuf.at[j],
            send_sem=rs_send.at[j], recv_sem=rs_recv.at[j],
            device_id=(sp_at(j), tp), device_id_type=MESH,
        )

    def slot_of(shard):
        behind = lax.rem(chip + chips - lax.div(shard, 2), chips)
        return 2 * behind + lax.rem(lax.rem(shard, 2) + core, 2)

    if flip:
        dpt[...] = dproj_ref[...].T
        per = feat // piece

        def share(j):
            dest = sp_at(j)
            x = gath[
                slot_of(lax.div(dest, per)), :, :,
                pl.ds(pl.multiple_of(lax.rem(dest, per) * piece, LANES), piece),
            ]
            return mm(dpt[...], x.reshape(rows, piece))

        def rs_start(j, _):
            sbuf[j] = share(j).astype(BF16)
            rs_copy(j).start()
            return 0

        lax.fori_loop(1, sp_n, rs_start, 0)
        own[...] = share(0)
    else:
        per = feat // piece

        def shares(shard, _):
            x = gath[slot_of(shard)].reshape(rows, feat)
            full = mm(x, dproj_ref[...], (((0,), (0,)), ((), ())))
            sbuf[pl.ds(shard * per, per)] = full.astype(BF16).reshape(per, piece, chan)
            return 0

        lax.fori_loop(0, tp_n, shares, 0)

        def rs_start(j, _):
            rs_copy(j).start()
            return 0

        lax.fori_loop(1, sp_n, rs_start, 0)
        own[...] = sbuf[sp].astype(F32)

    def ag_drain(c, _):
        for j in range(chips):
            if j:
                cross(j, c).wait_send()
            inside(j, c).wait_send()
        return 0

    lax.fori_loop(0, chunks, ag_drain, 0)

    def rs_wait(j, _):
        rs_copy(j).wait()
        return 0

    lax.fori_loop(1, sp_n, rs_wait, 0)
    height = own.shape[0]
    tile = min(32, height)

    def add(i, _):
        at = pl.ds(pl.multiple_of(i * tile, tile), tile)

        def more(j, acc):
            return acc + rbuf[j, at, :].astype(F32)

        own[at, :] = lax.fori_loop(1, sp_n, more, own[at, :])
        return 0

    lax.fori_loop(0, height // tile, add, 0)
    dw_ref[...] = own[...].T if flip else own[...]


def per_device(
    tokens, proj_weight, gate_weight, conv_weight, recur_weight, input_weight, decay_param, out_grad
):
    sp_n = lax.axis_size("sp")
    tp_n = lax.axis_size("tp")
    rows, feat = tokens.shape
    width, chan = proj_weight.shape
    sub_rows = rows // SUBS
    chunks = sub_rows // STEP
    halves = chan // LANES
    pitch = sub_rows + PAD
    piece = width // sp_n
    box = (chan, piece) if piece % LANES == 0 else (piece, chan)
    V = pltpu.VMEM
    DMA = pltpu.SemaphoreType.DMA
    tall = V((halves, SUBS * pitch, LANES), F32)
    small = V((PAD, chan), F32)
    any_space = pl.BlockSpec(memory_space=pl.ANY)
    in_vmem = pl.BlockSpec(memory_space=V)
    return pl.pallas_call(
        functools.partial(kernel, sp_n=sp_n, tp_n=tp_n),
        out_shape=(
            jax.ShapeDtypeStruct((rows, chan), BF16),
            jax.ShapeDtypeStruct((rows, chan), BF16),
            jax.ShapeDtypeStruct((piece, chan), F32),
        ),
        in_specs=[any_space] * 3 + [in_vmem] * 4 + [any_space],
        out_specs=(in_vmem,) * 3,
        scratch_shapes=[
            V((tp_n, SUBS, sub_rows, feat), BF16),
            V((width, chan), BF16),
            V((width, chan), BF16),
            V((rows, chan), BF16),
            V((chan, 2 * chan), BF16),
            V((SUBS, pitch, chan), F32),
            V((SUBS, sub_rows, chan), F32),
            V((SUBS * STEP, 2 * chan), F32),
        ] + [tall] * 13 + [
            V((3, SUBS, chan), F32),
            V((SUBS, 1, chan), F32),
            V((SUBS, 1, chan), F32),
            V((1, chan), F32),
            V((4, chan), F32),
            small,
            small,
            small,
            V((sp_n, PAD, chan), F32),
            V((max(SUBS * STEP, sub_rows), 2 * chan), BF16),
            V((rows + PAD, chan), F32),
            small,
            V((chan, rows), BF16),
            V((sp_n,) + box, BF16),
            V((sp_n,) + box, BF16),
            V(box, F32),
            DMA((4,)),
            DMA((tp_n, chunks)), DMA((tp_n, chunks)),
            DMA, DMA,
            DMA((sp_n,)), DMA((sp_n,)),
            DMA, DMA,
            DMA((sp_n,)), DMA((sp_n,)),
        ],
        compiler_params=pltpu.CompilerParams(
            collective_id=0, has_side_effects=True, vmem_limit_bytes=56 * 1024 * 1024
        ),
    )(
        tokens.reshape(SUBS, sub_rows, feat), proj_weight, gate_weight, conv_weight,
        recur_weight, input_weight, decay_param.reshape(1, -1), out_grad,
    )


def solution(mesh):
    in_specs = (P("sp", "tp"), P(None, "tp"), P(None, "tp"), P(), P(), P(), P(), P("sp", "tp"))
    out_specs = (P("sp", "tp"), P("sp", "tp"), P("sp", "tp"))
    return jax.shard_map(
        per_device, mesh=mesh, in_specs=in_specs, out_specs=out_specs, check_vma=False
    )
```

time: 447 us -> 65.6 us (0.15)
  the two profiles are of different devices: /device:TPU:0 before, /device:TPU:13 now
where the time goes in v1:
time: 65.6 us; the launch traced here: 65.4 us
  Pallas kernels  61.1 us (93%)
  local copies, waits for them, and re-layouts  3.61 us (6%)
    pallas_call x1, Pallas kernels, per_device(): pl.pallas_call(functools.partial(kernel, sp_n=sp_n, tp_n=tp_n), out_shape...  61.1 us
    unnamed x7, local copies, waits for them, and re-layouts  3.61 us

profile of v1, /device:TPU:13, one launch (start us, length us, event | category | flops | bytes accessed | tf_op | source)
XLA Modules:
  0.0 65.4 jit_solution(5974687220164139100)
XLA Ops:
  0.6 61.1 %shard_map.103 = (bf16[768,256]{1,0:T(8,128)(2,1)}, bf16[768,256]{1,0:T(8,128)(2,1)}, f32[256,256]{1,0:T(8,128)}) custom-call(bf16[8,96,512]{2,1,0:T(8,128)(2,1)} %bitcast.2, bf16[2048,256]{1,0:T(8,128)(2,1)} %wp_hbm.1, bf16[2048,256]{1,0:T(8,128)(2,1)} %wg_hbm.1, f32[4,1024]{1,0:T(4,128)} %cw_ref.1, bf16[16,64,64]{2,1,0:T(8,128)(2,1)} %wr_ref.1, ...), custom_call_target="tpu_custom_call" | custom-call | tf_op jit(solution)/shard_map/pallas_call | solution.py:463
  61.8 0.0 copy-start
  61.8 1.8 %copy.14 = bf16[768,256]{1,0:T(8,128)(2,1)} copy(bf16[768,256]{1,0:T(8,128)(2,1)} %get-tuple-element.6) | data formatting | bytes 786432
  63.6 0.0 copy-done
  63.6 0.0 copy-start.1
  63.6 0.7 %copy.15 = bf16[768,256]{1,0:T(8,128)(2,1)} copy(bf16[768,256]{1,0:T(8,128)(2,1)S(1)} %copy-done) | data formatting | bytes 786432
  64.3 0.3 copy-done.1
  64.7 0.7 %copy.16 = f32[256,256]{1,0:T(8,128)} copy(f32[256,256]{1,0:T(8,128)S(1)} %copy-done.1) | data formatting | bytes 524288
Async XLA Ops:
  61.8 1.8 %copy-start = (bf16[768,256]{1,0:T(8,128)(2,1)S(1)}, bf16[768,256]{1,0:T(8,128)(2,1)}, u32[]{:S(2)}) copy-start(bf16[768,256]{1,0:T(8,128)(2,1)} %get-tuple-element.7) | copy-start | bytes 1179652
  63.6 1.1 %copy-start.1 = (f32[256,256]{1,0:T(8,128)S(1)}, f32[256,256]{1,0:T(8,128)}, u32[]{:S(2)}) copy-start(f32[256,256]{1,0:T(8,128)} %get-tuple-element.8) | copy-start | bytes 786436

commit v2 on v1

--- a/solution.py
+++ b/solution.py
@@ -361,40 +361,69 @@
     lax.fori_loop(0, rows // STEP, unconv, 0, unroll=4)
 
     piece = feat * tp_n // sp_n
-    flip = piece % LANES == 0
-
-    def rs_copy(j):
-        return pltpu.make_async_remote_copy(
-            src_ref=sbuf.at[j if flip else sp_at(j)], dst_ref=rbuf.at[j],
-            send_sem=rs_send.at[j], recv_sem=rs_recv.at[j],
-            device_id=(sp_at(j), tp), device_id_type=MESH,
-        )
+    per = feat // piece
+    paired = piece % LANES == 0 and sp_n % 2 == 0
+    duos = sp_n // 2
+    side = lax.rem(sp, 2)
+    duo = lax.div(sp, 2)
 
     def slot_of(shard):
         behind = lax.rem(chip + chips - lax.div(shard, 2), chips)
         return 2 * behind + lax.rem(lax.rem(shard, 2) + core, 2)
 
-    if flip:
+    def rs_move(source, landing, target):
+        return pltpu.make_async_remote_copy(
+            src_ref=sbuf.at[source], dst_ref=rbuf.at[landing],
+            send_sem=rs_send.at[landing], recv_sem=rs_recv.at[landing],
+            device_id=(target, tp), device_id_type=MESH,
+        )
+
+    def rs_near(m):
+        return rs_move(duos + m, duos + m, sp + 1 - 2 * side)
+
+    def rs_far(m):
+        if paired:
+            return rs_move(m, m, lax.rem(duo + m, duos) * 2 + side)
+        return rs_move(sp_at(m), m, sp_at(m))
+
+    if paired:
         dpt[...] = dproj_ref[...].T
-        per = feat // piece
-
-        def share(j):
-            dest = sp_at(j)
+
+        def share(m, half):
+            dest = lax.rem(duo + m, duos) * 2 + half
             x = gath[
                 slot_of(lax.div(dest, per)), :, :,
                 pl.ds(pl.multiple_of(lax.rem(dest, per) * piece, LANES), piece),
             ]
             return mm(dpt[...], x.reshape(rows, piece))
 
-        def rs_start(j, _):
-            sbuf[j] = share(j).astype(BF16)
-            rs_copy(j).start()
-            return 0
-
-        lax.fori_loop(1, sp_n, rs_start, 0)
-        own[...] = share(0)
+        def near_start(i, _):
+            m = lax.rem(i + 1, duos)
+            sbuf[duos + m] = share(m, 1 - side).astype(BF16)
+            rs_near(m).start()
+            return 0
+
+        lax.fori_loop(0, duos, near_start, 0)
+
+        def far_start(m, _):
+            own[...] = share(m, side)
+            rs_near(m).wait_recv()
+            sbuf[m] = (own[...] + rbuf[duos + m].astype(F32)).astype(BF16)
+            rs_far(m).start()
+            return 0
+
+        lax.fori_loop(1, duos, far_start, 0)
+        own[...] = share(0, side)
+        rs_near(0).wait_recv()
+        own[...] += rbuf[duos].astype(F32)
+
+        def near_drain(m, _):
+            rs_near(m).wait_send()
+            return 0
+
+        lax.fori_loop(0, duos, near_drain, 0)
+        peers = duos
     else:
-        per = feat // piece
 
         def shares(shard, _):
             x = gath[slot_of(shard)].reshape(rows, feat)
@@ -404,12 +433,13 @@
 
         lax.fori_loop(0, tp_n, shares, 0)
 
-        def rs_start(j, _):
-            rs_copy(j).start()
-            return 0
-
-        lax.fori_loop(1, sp_n, rs_start, 0)
+        def far_start(m, _):
+            rs_far(m).start()
+            return 0
+
+        lax.fori_loop(1, sp_n, far_start, 0)
         own[...] = sbuf[sp].astype(F32)
+        peers = sp_n
 
     def ag_drain(c, _):
         for j in range(chips):
@@ -421,10 +451,10 @@
     lax.fori_loop(0, chunks, ag_drain, 0)
 
     def rs_wait(j, _):
-        rs_copy(j).wait()
-        return 0
-
-    lax.fori_loop(1, sp_n, rs_wait, 0)
+        rs_far(j).wait()
+        return 0
+
+    lax.fori_loop(1, peers, rs_wait, 0)
     height = own.shape[0]
     tile = min(32, height)
 
@@ -434,11 +464,25 @@
         def more(j, acc):
             return acc + rbuf[j, at, :].astype(F32)
 
-        own[at, :] = lax.fori_loop(1, sp_n, more, own[at, :])
+        own[at, :] = lax.fori_loop(1, peers, more, own[at, :])
         return 0
 
     lax.fori_loop(0, height // tile, add, 0)
-    dw_ref[...] = own[...].T if flip else own[...]
+    dw_ref[...] = own[...].T if paired else own[...]
+
+
+def emit(*refs):
+    sources, targets, rooms = refs[0:3], refs[3:6], refs[6:9]
+    in_sem, out_sem = refs[9:]
+    ins = [pltpu.make_async_copy(sources[i], rooms[i], in_sem.at[i]) for i in range(3)]
+    outs = [pltpu.make_async_copy(rooms[i], targets[i], out_sem.at[i]) for i in range(3)]
+    for item in ins:
+        item.start()
+    for i in range(3):
+        ins[i].wait()
+        outs[i].start()
+    for item in outs:
+        item.wait()
 
 
 def per_device(
@@ -453,14 +497,14 @@
     halves = chan // LANES
     pitch = sub_rows + PAD
     piece = width // sp_n
-    box = (chan, piece) if piece % LANES == 0 else (piece, chan)
+    box = (chan, piece) if piece % LANES == 0 and sp_n % 2 == 0 else (piece, chan)
     V = pltpu.VMEM
     DMA = pltpu.SemaphoreType.DMA
     tall = V((halves, SUBS * pitch, LANES), F32)
     small = V((PAD, chan), F32)
     any_space = pl.BlockSpec(memory_space=pl.ANY)
     in_vmem = pl.BlockSpec(memory_space=V)
-    return pl.pallas_call(
+    results = pl.pallas_call(
         functools.partial(kernel, sp_n=sp_n, tp_n=tp_n),
         out_shape=(
             jax.ShapeDtypeStruct((rows, chan), BF16),
@@ -509,6 +553,14 @@
         tokens.reshape(SUBS, sub_rows, feat), proj_weight, gate_weight, conv_weight,
         recur_weight, input_weight, decay_param.reshape(1, -1), out_grad,
     )
+    shapes = [jax.ShapeDtypeStruct(r.shape, r.dtype) for r in results]
+    return pl.pallas_call(
+        emit,
+        out_shape=tuple(shapes),
+        in_specs=[any_space] * 3,
+        out_specs=(any_space,) * 3,
+        scratch_shapes=[V(s.shape, s.dtype) for s in shapes] + [DMA((3,)), DMA((3,))],
+    )(*results)
 
 
 def solution(mesh):

time: 65.6 us -> 57.8 us (0.88)
  the two profiles are of different devices: /device:TPU:13 before, /device:TPU:0 now
where the time goes in v2:
time: 57.8 us; the launch traced here: 57.6 us
  Pallas kernels  57 us (99%)
  between operations  0.64 us (1%)
    pallas_call x1, Pallas kernels, per_device(): pl.pallas_call(functools.partial(kernel, sp_n=sp_n, tp_n=tp_n), out_shape...  54.9 us
    pallas_call x1, Pallas kernels, per_device(): pl.pallas_call(emit, out_shape=tuple(shapes), in_specs=[any_space] * 3, o...  2.01 us

profile of v2, /device:TPU:0, one launch (start us, length us, event | category | flops | bytes accessed | tf_op | source)
XLA Modules:
  0.0 57.6 jit_solution(11412658849753267120)
XLA Ops:
  0.6 54.9 %shard_map.103 = (bf16[768,256]{1,0:T(8,128)(2,1)}, bf16[768,256]{1,0:T(8,128)(2,1)}, f32[256,256]{1,0:T(8,128)}) custom-call(bf16[8,96,512]{2,1,0:T(8,128)(2,1)} %bitcast.2, bf16[2048,256]{1,0:T(8,128)(2,1)} %wp_hbm.1, bf16[2048,256]{1,0:T(8,128)(2,1)} %wg_hbm.1, f32[4,1024]{1,0:T(4,128)} %cw_ref.1, bf16[16,64,64]{2,1,0:T(8,128)(2,1)} %wr_ref.1, ...), custom_call_target="tpu_custom_call" | custom-call | tf_op jit(solution)/shard_map/pallas_call | solution.py:507
  55.6 2.0 %shard_map.104 = (bf16[768,256]{1,0:T(8,128)(2,1)}, bf16[768,256]{1,0:T(8,128)(2,1)}, f32[256,256]{1,0:T(8,128)}) custom-call(bf16[768,256]{1,0:T(8,128)(2,1)} %get-tuple-element.6.refs_0_, bf16[768,256]{1,0:T(8,128)(2,1)} %get-tuple-element.7.refs_1_, f32[256,256]{1,0:T(8,128)} %get-tuple-element.8.refs_2_), custom_call_target="tpu_custom_call" | custom-call | tf_op jit(solution)/shard_map/pallas_call | solution.py:557

commit v3 on v2

--- a/solution.py
+++ b/solution.py
@@ -12,6 +12,7 @@
 scale_floor = 0.0001
 
 SUBS = 8
+PARTS = 4
 STEP = 16
 LANES = 128
 PAD = 8
@@ -26,13 +27,13 @@
 
 def kernel(
     tok_hbm, wp_hbm, wg_hbm, cw_ref, wr_ref, wi_ref, dp_ref, og_hbm,
-    dproj_ref, dgate_ref, dw_ref,
+    dproj_hbm, dgate_hbm, dw_ref,
     gath, wp, wg, og, wblk, proj, gin, pre,
     dec, drv, dgr, qg, ro_s, io_s, cv_s, sc_s, rs_s, xp, cp, gs, as_,
     ends, carry_k, carry_l, slope_s, taps_s,
     halo_out, halo_in, car_out, car_in, dri, dc, dc_in, dpt, sbuf, rbuf, own,
     loc_sem, ag_send, ag_recv, halo_send, halo_recv, car_send, car_recv,
-    dc_send, dc_recv, rs_send, rs_recv,
+    dc_send, dc_recv, rs_send, rs_recv, dproj_ref, dgate_ref, out_sem,
     *, sp_n, tp_n,
 ):
     sp = lax.axis_index("sp")
@@ -360,6 +361,13 @@
 
     lax.fori_loop(0, rows // STEP, unconv, 0, unroll=4)
 
+    leave = [
+        pltpu.make_async_copy(dproj_ref, dproj_hbm, out_sem.at[0]),
+        pltpu.make_async_copy(dgate_ref, dgate_hbm, out_sem.at[1]),
+    ]
+    for item in leave:
+        item.start()
+
     piece = feat * tp_n // sp_n
     per = feat // piece
     paired = piece % LANES == 0 and sp_n % 2 == 0
@@ -371,20 +379,24 @@
         behind = lax.rem(chip + chips - lax.div(shard, 2), chips)
         return 2 * behind + lax.rem(lax.rem(shard, 2) + core, 2)
 
-    def rs_move(source, landing, target):
+    cuts = PARTS if paired else 1
+    slab = own.shape[0] // cuts
+
+    def rs_move(source, landing, target, cut):
+        across = pl.ds(cut * slab, slab)
         return pltpu.make_async_remote_copy(
-            src_ref=sbuf.at[source], dst_ref=rbuf.at[landing],
-            send_sem=rs_send.at[landing], recv_sem=rs_recv.at[landing],
+            src_ref=sbuf.at[source, across], dst_ref=rbuf.at[landing, across],
+            send_sem=rs_send.at[landing, cut], recv_sem=rs_recv.at[landing, cut],
             device_id=(target, tp), device_id_type=MESH,
         )
 
-    def rs_near(m):
-        return rs_move(duos + m, duos + m, sp + 1 - 2 * side)
-
-    def rs_far(m):
+    def rs_near(m, cut):
+        return rs_move(duos + m, duos + m, sp + 1 - 2 * side, cut)
+
+    def rs_far(m, cut):
         if paired:
-            return rs_move(m, m, lax.rem(duo + m, duos) * 2 + side)
-        return rs_move(sp_at(m), m, sp_at(m))
+            return rs_move(m, m, lax.rem(duo + m, duos) * 2 + side, cut)
+        return rs_move(sp_at(m), m, sp_at(m), cut)
 
     if paired:
         dpt[...] = dproj_ref[...].T
@@ -400,25 +412,30 @@
         def near_start(i, _):
             m = lax.rem(i + 1, duos)
             sbuf[duos + m] = share(m, 1 - side).astype(BF16)
-            rs_near(m).start()
+            for cut in range(cuts):
+                rs_near(m, cut).start()
             return 0
 
         lax.fori_loop(0, duos, near_start, 0)
 
         def far_start(m, _):
             own[...] = share(m, side)
-            rs_near(m).wait_recv()
-            sbuf[m] = (own[...] + rbuf[duos + m].astype(F32)).astype(BF16)
-            rs_far(m).start()
+            for cut in range(cuts):
+                across = pl.ds(cut * slab, slab)
+                rs_near(m, cut).wait_recv()
+                sbuf[m, across] = (own[across] + rbuf[duos + m, across].astype(F32)).astype(BF16)
+                rs_far(m, cut).start()
             return 0
 
         lax.fori_loop(1, duos, far_start, 0)
         own[...] = share(0, side)
-        rs_near(0).wait_recv()
+        for cut in range(cuts):
+            rs_near(0, cut).wait_recv()
         own[...] += rbuf[duos].astype(F32)
 
         def near_drain(m, _):
-            rs_near(m).wait_send()
+            for cut in range(cuts):
+                rs_near(m, cut).wait_send()
             return 0
 
         lax.fori_loop(0, duos, near_drain, 0)
@@ -434,7 +451,7 @@
         lax.fori_loop(0, tp_n, shares, 0)
 
         def far_start(m, _):
-            rs_far(m).start()
+            rs_far(m, 0).start()
             return 0
 
         lax.fori_loop(1, sp_n, far_start, 0)
@@ -451,7 +468,8 @@
     lax.fori_loop(0, chunks, ag_drain, 0)
 
     def rs_wait(j, _):
-        rs_far(j).wait()
+        for cut in range(cuts):
+            rs_far(j, cut).wait()
         return 0
 
     lax.fori_loop(1, peers, rs_wait, 0)
@@ -468,6 +486,8 @@
         return 0
 
     lax.fori_loop(0, height // tile, add, 0)
+    for item in leave:
+        item.wait()
     dw_ref[...] = own[...].T if paired else own[...]
 
 
@@ -512,7 +532,7 @@
             jax.ShapeDtypeStruct((piece, chan), F32),
         ),
         in_specs=[any_space] * 3 + [in_vmem] * 4 + [any_space],
-        out_specs=(in_vmem,) * 3,
+        out_specs=(any_space, any_space, in_vmem),
         scratch_shapes=[
             V((tp_n, SUBS, sub_rows, feat), BF16),
             V((width, chan), BF16),
@@ -544,7 +564,10 @@
             DMA, DMA,
             DMA((sp_n,)), DMA((sp_n,)),
             DMA, DMA,
-            DMA((sp_n,)), DMA((sp_n,)),
+            DMA((sp_n, PARTS)), DMA((sp_n, PARTS)),
+            V((rows, chan), BF16),
+            V((rows, chan), BF16),
+            DMA((2,)),
         ],
         compiler_params=pltpu.CompilerParams(
             collective_id=0, has_side_effects=True, vmem_limit_bytes=56 * 1024 * 1024

time: 57.8 us -> 56 us (0.969)
  Pallas kernels: 57 us -> 55.2 us
    pallas_call x1, Pallas kernels: 54.9 us -> 53.2 us  [per_device(): pl.pallas_call(functools.partial(kernel, sp_n=sp_n, tp_n=tp_n), out_shape...]
where the time goes in v3:
time: 56 us; the launch traced here: 55.9 us
  Pallas kernels  55.2 us (99%)
  between operations  0.64 us (1%)
    pallas_call x1, Pallas kernels, per_device(): pl.pallas_call(functools.partial(kernel, sp_n=sp_n, tp_n=tp_n), out_shape...  53.2 us
    pallas_call x1, Pallas kernels, per_device(): pl.pallas_call(emit, out_shape=tuple(shapes), in_specs=[any_space] * 3, o...  2.01 us

profile of v3, /device:TPU:0, one launch (start us, length us, event | category | flops | bytes accessed | tf_op | source)
XLA Modules:
  0.0 55.9 jit_solution(6167991420653293397)
XLA Ops:
  0.6 53.2 %shard_map.103 = (bf16[768,256]{1,0:T(8,128)(2,1)}, bf16[768,256]{1,0:T(8,128)(2,1)}, f32[256,256]{1,0:T(8,128)}) custom-call(bf16[8,96,512]{2,1,0:T(8,128)(2,1)} %bitcast.2, bf16[2048,256]{1,0:T(8,128)(2,1)} %wp_hbm.1, bf16[2048,256]{1,0:T(8,128)(2,1)} %wg_hbm.1, f32[4,1024]{1,0:T(4,128)} %cw_ref.1, bf16[16,64,64]{2,1,0:T(8,128)(2,1)} %wr_ref.1, ...), custom_call_target="tpu_custom_call" | custom-call | tf_op jit(solution)/shard_map/pallas_call | solution.py:527
  53.9 2.0 %shard_map.104 = (bf16[768,256]{1,0:T(8,128)(2,1)}, bf16[768,256]{1,0:T(8,128)(2,1)}, f32[256,256]{1,0:T(8,128)}) custom-call(bf16[768,256]{1,0:T(8,128)(2,1)} %get-tuple-element.6.refs_0_, bf16[768,256]{1,0:T(8,128)(2,1)} %get-tuple-element.7.refs_1_, f32[256,256]{1,0:T(8,128)} %get-tuple-element.8.refs_2_), custom_call_target="tpu_custom_call" | custom-call | tf_op jit(solution)/shard_map/pallas_call | solution.py:580
